TPU v7x, 512 devices: a whole 4x4x16 slice. The times are simulated.
512 devices in a mesh: gr: 2 (over z_hi), fs: 32 (over z_lo, y), tp: 8 (over x, core).
Axes of the slice: x: 4, y: 4, z: 16 (z_hi: 2, z_lo: 8; z = z_hi * 8 + z_lo), core: 2. Of those that a mesh axis runs over, the one named last changes fastest.
Arguments:
- tokens: bfloat16 [12288, 2048], P(('gr', 'fs')), may hold values from -6 to 6
- routes: int32 [12288, 8], P(('gr', 'fs')), may hold values from 0 to 63, all different within a row; in each aligned block of 192 rows (0 to 191, 192 to 383, ...) at most 36 rows name the same one
- route_weight: float32 [12288, 8], P(('gr', 'fs')), may hold values from 0.05 to 0.6
- norm_gain: float32 [2048], replicated, may hold values from 0.1 to 1.9
- gate_experts: float32 [2, 32, 512, 2048], P('gr', None, 'fs', 'tp'), may hold values from -0.125 to 0.125
- up_experts: float32 [2, 32, 512, 2048], P('gr', None, 'fs', 'tp'), may hold values from -0.125 to 0.125
- down_experts: float32 [2, 32, 512, 2048], P('gr', None, 'fs', 'tp'), may hold values from -0.25 to 0.25
- gate_shared: float32 [2048, 512], P('fs', 'tp'), may hold values from -0.125 to 0.125
- up_shared: float32 [2048, 512], P('fs', 'tp'), may hold values from -0.125 to 0.125
- down_shared: float32 [512, 2048], P('fs', 'tp'), may hold values from -0.25 to 0.25
Outputs:
- mixed: bfloat16 [12288, 2048], P(('gr', 'fs'), 'tp')
- gate_served: bfloat16 [2, 32, 512, 2048], P(None, 'fs', 'tp')
- up_served: bfloat16 [2, 32, 512, 2048], P(None, 'fs', 'tp')
- down_served: bfloat16 [2, 32, 512, 2048], P(None, 'fs', None, 'tp')
- gate_shared_served: bfloat16 [2048, 512], P(None, 'tp')
- up_shared_served: bfloat16 [2048, 512], P(None, 'tp')
- down_shared_served: bfloat16 [512, 2048], P(None, 'tp')
Inputs may be any that keep to these rules, and one draw needn't show every extreme that they name: `routes`: each row names 8 different experts; within the 192 rows of one device no expert is named by more than 36 rows, and some expert reaches 36.
All inputs are finite; a program needn't handle non-finite values.
Results may differ from a plain program's by a relative error of at most 0.0084.
Values may be sent and summed in bfloat16 or wider, within the bound.
No kernel may reach another device: no remote copies, remote signals or barrier semaphores. Data moves between devices by JAX's collectives and lax.ppermute only.
A program may use at most 128 MiB of HBM per device.

v0:
```python
import jax
import jax.numpy as jnp
from jax import lax
from jax.sharding import PartitionSpec as P

EXP_HALF = 1
EPS = 1e-06


def sent_to_all(shard, axis):
    copies = jnp.broadcast_to(shard, (lax.axis_size(axis), *shard.shape))
    return lax.all_to_all(copies, axis, split_axis=0, concat_axis=0, tiled=True)


def joined_along(parts, dim):
    dims = list(parts.shape[1:])
    dims[dim] *= parts.shape[0]
    return jnp.moveaxis(parts, 0, dim).reshape(dims)


def collect(shard, axis, dim):
    parts = sent_to_all(shard, axis)
    return joined_along(parts, dim)


def side_by_side(arrays, axis, dim, along):
    widths = [a.shape[along] for a in arrays]
    both = jnp.concatenate(arrays, axis=along)
    whole = collect(both, axis, dim)
    return tuple(jnp.split(whole, [sum(widths[:k]) for k in range(1, len(widths))], axis=along))


def sent_together(arrays, axis, split_dim, concat_dim, along):
    widths = [a.shape[along] for a in arrays]
    both = jnp.concatenate(arrays, axis=along)
    whole = lax.all_to_all(both, axis, split_axis=split_dim, concat_axis=concat_dim, tiled=True)
    return tuple(jnp.split(whole, [sum(widths[:k]) for k in range(1, len(widths))], axis=along))


def in_one_piece(arrays, axis, dim, along):
    both = jnp.concatenate(arrays, axis=along)
    whole, at, gathered = (lax.all_gather(both, axis, axis=dim, tiled=True), 0, [])
    for a in arrays:
        gathered.append(lax.slice_in_dim(whole, at, at + a.shape[along], axis=along))
        at += a.shape[along]
    return tuple(gathered)


def on_device(
    tokens,
    routes,
    route_weight,
    norm_gain,
    gate_experts,
    up_experts,
    down_experts,
    gate_shared,
    up_shared,
    down_shared,
):
    bf = jnp.bfloat16
    f32 = jnp.float32
    n_fs = lax.axis_size("fs")
    n_gr = lax.axis_size("gr")
    n_tp = lax.axis_size("tp")
    fs_index = lax.axis_index("fs")
    cols_here = gate_experts.shape[3]
    gain_cols = lax.dynamic_slice_in_dim(norm_gain, lax.axis_index("tp") * cols_here, cols_here, 0)
    gate_local = (gate_experts * gain_cols[None, None, None, :]).astype(bf)
    up_local = (up_experts * gain_cols[None, None, None, :]).astype(bf)
    down_local = down_experts.astype(bf)
    shared_here = gate_shared.shape[0]
    gain_shared = lax.dynamic_slice_in_dim(norm_gain, fs_index * shared_here, shared_here, 0)
    gate_sh_local = (gate_shared * gain_shared[:, None]).astype(bf)
    up_sh_local = (up_shared * gain_shared[:, None]).astype(bf)
    down_sh_local = down_shared.astype(bf)
    halves = side_by_side((gate_local, up_local, down_local), "gr", 0, 1)
    gate_cols, up_cols, down_w = sent_together((halves[0], halves[1], halves[2]), "fs", 1, 2, 0)
    gate_w, up_w = sent_together((gate_cols, up_cols), "tp", 2, 3, 0)
    gate_sw, up_sw, down_sw = (
        *in_one_piece((gate_sh_local, up_sh_local), "fs", 0, 1),
        lax.all_gather(down_sh_local, "fs", axis=0, tiled=True),
    )
    values = tokens.astype(f32)
    normed = (values * lax.rsqrt(jnp.mean(values * values, axis=-1, keepdims=True) + EPS)).astype(
        bf
    )
    tok_count, top = routes.shape
    width = tokens.shape[1]
    per_group = gate_experts.shape[1]
    count = per_group * n_gr
    capacity = (3 * tok_count * top + 2 * count - 1) // (2 * count)
    flat_e = routes.reshape(-1)
    onehot = (flat_e[:, None] == jnp.arange(count, dtype=jnp.int32)[None, :]).astype(jnp.int32)
    ranks = jnp.sum(jnp.cumsum(onehot, axis=0) * onehot, axis=1) - 1
    group_of = flat_e // per_group
    within = flat_e % per_group
    target = within // EXP_HALF
    local_k = within % EXP_HALF
    slot = ((target * n_gr + group_of) * EXP_HALF + local_k) * capacity + ranks
    total_slots = n_fs * n_gr * EXP_HALF * capacity
    repeated = jnp.repeat(normed, top, axis=0)
    send = jnp.zeros((total_slots, width), bf).at[slot].set(repeated)
    send = send.reshape(n_fs, n_gr, EXP_HALF, capacity, width)
    cols = width // n_tp
    send = lax.dynamic_slice_in_dim(send, lax.axis_index("tp") * cols, cols, 4)
    received = lax.all_to_all(send, "fs", split_axis=0, concat_axis=0, tiled=True)
    received = lax.all_gather(received, "tp", axis=4, tiled=True)
    gate = jnp.einsum("sgkcd,gkfd->sgkcf", received, gate_w, preferred_element_type=f32)
    upper = jnp.einsum("sgkcd,gkfd->sgkcf", received, up_w, preferred_element_type=f32)
    hidden = (jax.nn.silu(gate) * upper).astype(bf)
    full_hidden = collect(hidden, "tp", 4)
    result = jnp.einsum(
        "sgkcf,gkfe->sgkce", full_hidden, down_w, preferred_element_type=f32
    ).astype(bf)
    returned = lax.all_to_all(result, "fs", split_axis=0, concat_axis=0, tiled=True)
    picked = returned.reshape(total_slots, cols)[slot].reshape(tok_count, top, cols)
    routed = jnp.einsum("tkc,tk->tc", picked.astype(f32), route_weight)
    shared_gate = jnp.dot(normed, gate_sw, preferred_element_type=f32)
    shared_up = jnp.dot(normed, up_sw, preferred_element_type=f32)
    shared_hidden = (jax.nn.silu(shared_gate) * shared_up).astype(bf)
    shared_full = collect(shared_hidden, "tp", 1)
    shared = jnp.dot(shared_full, down_sw, preferred_element_type=f32)
    mixed = (routed + shared).astype(bf)
    return (mixed, gate_w, up_w, down_w, gate_sw, up_sw, down_sw)


def solution(mesh):
    return jax.shard_map(
        on_device,
        mesh=mesh,
        in_specs=(
            P(("gr", "fs"), None),
            P(("gr", "fs"), None),
            P(("gr", "fs"), None),
            P(),
            P("gr", None, "fs", "tp"),
            P("gr", None, "fs", "tp"),
            P("gr", None, "fs", "tp"),
            P("fs", "tp"),
            P("fs", "tp"),
            P("fs", "tp"),
        ),
        out_specs=(
            P(("gr", "fs"), "tp"),
            P(None, "fs", "tp", None),
            P(None, "fs", "tp", None),
            P(None, "fs", None, "tp"),
            P(None, "tp"),
            P(None, "tp"),
            P(None, "tp"),
        ),
        check_vma=False,
    )
```

profile of v0, /device:TPU:1, one launch (start us, length us, event | category | flops | bytes accessed | tf_op | source)
XLA Modules:
  0.0 694.6 jit_solution(2489082165161462181)
XLA Ops:
  8.4 1.4 fusion.8
  10.1 18.1 %reduce-window.6 = s32[64,12,128]{2,1,0:T(8,128)S(1)} reduce-window(s32[64,12,128]{2,1,0:T(8,128)S(1)} %fusion.32, s32[]{:T(128)} %constant.70.clone.1), window={size=1x1x128 pad=0_0x0_0x127_0}, to_apply=%region_0.0 | reduce-window | flops 12484608 | bytes 786436 | tf_op jit(solution)/shard_map/reduce-window
  29.3 14.6 %scatter_custom_fusion = bf16[2304,2048]{1,0:T(8,128)(2,1)} fusion(s32[1536]{0:T(1024)S(1)} %fusion.35, bf16[]{:T(256)} %constant.72.clone.1, bf16[192,2048]{1,0:T(8,128)(2,1)S(1)} %fusion.9), kind=kCustom, calls=%fused_computation.6 | custom fusion | bytes 10223618 | tf_op jit(solution)/shard_map/scatter | solution.py:103
  43.9 13.1 %reshape.234 = bf16[32,2,1,36,2048]{4,3,1,0,2:T(8,128)(2,1)} reshape(bf16[2304,2048]{1,0:T(8,128)(2,1)} %scatter_custom_fusion) | data formatting | bytes 18874368 | tf_op jit(solution)/shard_map/reshape | solution.py:104
  57.0 1.4 constant_dynamic-slice_fusion
  59.3 73.5 %all_to_all.49 = bf16[32,2,1,36,256]{4,1,3,2,0:T(2,128)(2,1)S(1)} all-to-all(bf16[32,2,1,36,256]{4,1,3,2,0:T(2,128)(2,1)S(1)} %copy.85), channel_id=1, replica_groups=mesh['gr'=2,'fs'=32,'tp'=8] {'fs'}, dimensions={0} | all-to-all | bytes 2359296 | tf_op jit(solution)/shard_map/all_to_all | solution.py:107
  132.8 1.3 copy.86
  135.6 42.3 %all_to_all.50 = bf16[2,1,96,16,256]{4,3,2,1,0:T(8,128)(2,1)S(1)} all-to-all(bf16[2,1,96,16,256]{4,3,2,1,0:T(8,128)(2,1)S(1)} %broadcast_in_dim.10), channel_id=1, replica_groups=mesh['gr'=2,'fs'=32,'tp'=8] {'gr'}, dimensions={0} | all-to-all | bytes 3145728 | tf_op jit(solution)/shard_map/all_to_all | solution.py:12
  178.3 122.1 %all_to_all.51 = bf16[6,32,16,256]{3,2,0,1:T(8,128)(2,1)S(1)} all-to-all(bf16[6,32,16,256]{3,2,0,1:T(8,128)(2,1)S(1)} %copy.73), channel_id=1, replica_groups=mesh['gr'=2,'fs'=32,'tp'=8] {'fs'}, dimensions={1} | all-to-all | bytes 3145728 | tf_op jit(solution)/shard_map/all_to_all | solution.py:36
  301.6 21.3 %all_to_all.52 = bf16[4,1,512,256]{3,0,1,2:T(4,128)(2,1)S(1)} all-to-all(bf16[4,1,512,256]{3,0,1,2:T(4,128)(2,1)S(1)} %copy.77), channel_id=1, replica_groups=mesh['gr'=2,'fs'=32,'tp'=8] {'tp'}, dimensions={2} | all-to-all | bytes 2097152 | tf_op jit(solution)/shard_map/all_to_all | solution.py:36
  326.7 5.9 fusion.11
  332.6 1.5 copy-done.12
  334.0 3.2 fusion.23
  337.4 3.0 broadcast_bitcast_fusion
  340.4 7.9 %reshape.268 = bf16[8,2,73728]{2,1,0:T(2,128)(2,1)} reshape(bf16[8,1,2,36,32,64]{5,4,3,2,1,0:T(8,128)(2,1)} %broadcast_bitcast_fusion) | data formatting | bytes 4718592
  348.3 5.3 all-to-all-start.4
  353.7 29.1 %all-to-all-done.4 = bf16[8,2,73728]{2,1,0:T(2,128)(2,1)} async-done(((bf16[8,2,73728]{2,1,0:T(2,128)(2,1)}), bf16[8,2,73728]{2,1,0:T(2,128)(2,1)}, u32[]{:S(2)}, u32[]{:S(2)}) %all-to-all-start.4) | async-done | bytes 2359328 | tf_op jit(solution)/shard_map/all_to_all | solution.py:12
  382.8 7.7 %reshape.269 = bf16[8,1,2,36,32,64]{5,4,3,2,1,0:T(8,128)(2,1)} reshape(bf16[8,2,73728]{2,1,0:T(2,128)(2,1)} %all-to-all-done.4) | data formatting | bytes 4718592
  390.5 3.1 bitcast_bitcast_fusion.1
  393.6 5.2 copy.105
  398.8 7.3 %reshape.264 = bf16[32,2,36,512]{3,2,0,1:T(8,128)(2,1)} reshape(bf16[32,2,1,36,8,64]{5,4,3,0,1,2:T(8,128)(2,1)} %copy.105) | data formatting | bytes 4718592 | tf_op jit(solution)/shard_map/reshape.37
  406.1 2.6 fusion.10
  408.7 2.2 copy.91
  410.9 5.6 all-to-all-start.5
  417.7 120.1 %all_gather.10 = bf16[2048,128]{1,0:T(8,128)(2,1)S(1)} all-gather(bf16[64,128]{1,0:T(8,128)(2,1)S(1)} %pad_maximum_fusion.2), channel_id=1, replica_groups=mesh['gr'=2,'fs'=32,'tp'=8] {'fs'}, dimensions={0}, use_global_device_ids=true | all-gather | bytes 540672 | tf_op jit(solution)/shard_map/all_gather | solution.py:42
  537.8 1.1 fusion.43
  538.9 1.9 copy.98
  540.8 1.9 copy.99
  542.8 100.0 %all_gather.11 = bf16[512,256]{1,0:T(8,128)(2,1)S(1)} all-gather(bf16[16,256]{1,0:T(8,128)(2,1)S(1)} %convert_element_type.64), channel_id=1, replica_groups=mesh['gr'=2,'fs'=32,'tp'=8] {'fs'}, dimensions={0}, use_global_device_ids=true | all-gather | bytes 270336 | tf_op jit(solution)/shard_map/all_gather | solution.py:82
  646.8 32.6 %all-to-all-start.6 = ((bf16[8,192,64]{1,2,0:T(8,128)(2,1)}), bf16[8,192,64]{1,2,0:T(8,128)(2,1)S(1)}, u32[]{:S(2)}, u32[]{:S(2)}) async-start(bf16[8,192,64]{1,2,0:T(8,128)(2,1)} %broadcast_in_dim.27), calls=%async_computation.6 | async-start | bytes 524288 | tf_op jit(solution)/shard_map/all_to_all | solution.py:12
  679.3 1.5 copy.92
  681.1 4.8 gather_fusion
  (82 shorter events, 17.6 us)
Async XLA Ops:
  7.2 2.6 copy-start.1
  7.2 319.5 %all-gather.2.cloned.1.call-start = ((), (), s32[]{:S(2)}) async-start(), calls=%async_computation.7 | async-start | bytes 11796480 | tf_op jit(solution)/shard_map/all_gather | solution.py:108
  132.8 1.3 copy-start.3
  134.0 1.0 copy-start.6
  134.0 1.2 copy-start.7
  326.7 5.9 copy-start.5
  326.7 7.3 %copy-start.12 = (bf16[32,2,1,36,2048]{4,3,0,1,2:T(8,128)(2,1)S(1)}, bf16[32,2,1,36,2048]{4,3,0,1,2:T(8,128)(2,1)}, u32[]{:S(2)}) copy-start(bf16[32,2,1,36,2048]{4,3,0,1,2:T(8,128)(2,1)} %all-gather.2.cloned.1.call-done) | copy-start | bytes 28311556
  348.3 34.4 %all-to-all-start.4 = ((bf16[8,2,73728]{2,1,0:T(2,128)(2,1)}), bf16[8,2,73728]{2,1,0:T(2,128)(2,1)}, u32[]{:S(2)}, u32[]{:S(2)}) async-start(bf16[8,2,73728]{2,1,0:T(2,128)(2,1)} %reshape.268), calls=%async_computation.4 | async-start | bytes 4718592 | tf_op jit(solution)/shard_map/all_to_all | solution.py:12
  353.7 52.5 %copy-start.4 = (bf16[2,32,16,256]{3,2,1,0:T(8,128)(2,1)}, bf16[2,32,16,256]{3,2,1,0:T(8,128)(2,1)S(1)}, u32[]{:S(2)}) copy-start(bf16[2,32,16,256]{3,2,1,0:T(8,128)(2,1)S(1)} %copy.107) | copy-start | bytes 1572868
  410.9 6.4 copy-start.10
  410.9 6.4 copy-start.11
  410.9 6.6 copy-start.8
  410.9 6.6 copy-start.9
  410.9 234.7 %all-to-all-start.5 = ((bf16[32,2,1,36,256]{4,1,3,2,0:T(2,128)(2,1)}), bf16[32,2,1,36,256]{4,1,3,2,0:T(2,128)(2,1)S(1)}, u32[]{:S(2)}, u32[]{:S(2)}) async-start(bf16[32,2,1,36,256]{4,1,3,2,0:T(2,128)(2,1)} %copy.91), calls=%async_computation.5 | async-start | bytes 2359296 | tf_op jit(solution)/shard_map/all_to_all | solution.py:116
  542.8 101.1 %copy-start.2 = (bf16[1,2,8,8,8,256]{5,4,3,2,1,0:T(8,128)(2,1)S(1)}, bf16[1,2,8,8,8,256]{5,4,3,2,1,0:T(8,128)(2,1)}, u32[]{:S(2)}) copy-start(bf16[1,2,8,8,8,256]{5,4,3,2,1,0:T(8,128)(2,1)} %get-tuple-element.35) | copy-start | bytes 1572868
  645.6 1.1 copy-start
  646.8 39.4 %all-to-all-start.6 = ((bf16[8,192,64]{1,2,0:T(8,128)(2,1)}), bf16[8,192,64]{1,2,0:T(8,128)(2,1)S(1)}, u32[]{:S(2)}, u32[]{:S(2)}) async-start(bf16[8,192,64]{1,2,0:T(8,128)(2,1)} %broadcast_in_dim.27), calls=%async_computation.6 | async-start | bytes 524288 | tf_op jit(solution)/shard_map/all_to_all | solution.py:12
Sparse Core Ops, SparseCore 0:
  134.2 66.9 all-gather.1
where the time goes:
time: 696 us; the launch traced here: 695 us
  blocking collectives  479 us (69%)
  local copies, waits for them, and re-layouts  93.5 us (13%)
  starting transfers between devices  43.5 us (6%)
  waiting for transfers between devices  29.1 us (4%)
  other arithmetic  20.9 us (3%)
  between operations  14.4 us (2%)
  matrix products  14 us (2%)
    all_to_all x2, blocking collectives, sent_together(): lax.all_to_all(both, axis, split_axis=split_dim, concat_axis=concat_dim,...  143 us
    all_gather x1, blocking collectives, in_one_piece(): lax.all_gather(both, axis, axis=dim, tiled=True)  120 us
    all_gather x1, blocking collectives, on_device(): lax.all_gather(down_sh_local, 'fs', axis=0, tiled=True)  100 us
    all_to_all x1, blocking collectives, on_device(): lax.all_to_all(send, 'fs', split_axis=0, concat_axis=0, tiled=True)  73.5 us
    all_to_all x1, blocking collectives, sent_to_all(): return lax.all_to_all(copies, axis, split_axis=0, concat_axis=0, tiled=True)  42.3 us
    all_to_all x2, starting transfers between devices, sent_to_all(): return lax.all_to_all(copies, axis, split_axis=0, concat_axis=0, tiled=True)  37.9 us
    all_to_all x2, waiting for transfers between devices, sent_to_all(): return lax.all_to_all(copies, axis, split_axis=0, concat_axis=0, tiled=True)  29.1 us
    unnamed x38, local copies, waits for them, and re-layouts  27.5 us
  transfers between devices with their start and end apart: 4, of which 1 were waited for; matrix products, arithmetic and copies ran while one was open for 3% of the time, Pallas kernels for 0%

commit v1 on v0

--- a/solution.py
+++ b/solution.py
@@ -79,7 +79,15 @@
     gate_w, up_w = sent_together((gate_cols, up_cols), "tp", 2, 3, 0)
     gate_sw, up_sw, down_sw = (
         *in_one_piece((gate_sh_local, up_sh_local), "fs", 0, 1),
-        lax.all_gather(down_sh_local, "fs", axis=0, tiled=True),
+        jnp.concatenate(
+            jax.lax.all_to_all(
+                jnp.stack([down_sh_local for _ in range(jax.lax.axis_size("fs"))], axis=0),
+                "fs",
+                0,
+                0,
+            ),
+            axis=0,
+        ),
     )
     values = tokens.astype(f32)
     normed = (values * lax.rsqrt(jnp.mean(values * values, axis=-1, keepdims=True) + EPS)).astype(

time: 696 us -> 595 us (0.85)
  blocking collectives: 479 us -> 379 us
    all_gather x1 -> x0, blocking collectives: 100 us -> none  [on_device(): lax.all_gather(down_sh_local, 'fs', axis=0, tiled=True)]
    all_to_all x2, starting transfers between devices: 37.9 us -> 24 us  [sent_to_all(): return lax.all_to_all(copies, axis, split_axis=0, concat_axis=0, tiled=True)]
    another operation x5 -> x6, local copies, waits for them, and re-layouts: 14.7 us -> 15.3 us
  transfers between devices with their start and end apart: 4 -> 5, of which waited for: 1 -> 1; matrix products, arithmetic and copies ran while one was open for 3% -> 9% of each run, Pallas kernels for 0% -> 0%
where the time goes in v1:
time: 595 us; the launch traced here: 593 us
  blocking collectives  379 us (64%)
  local copies, waits for them, and re-layouts  94.3 us (16%)
  starting transfers between devices  41.7 us (7%)
  waiting for transfers between devices  29.2 us (5%)
  other arithmetic  20.9 us (4%)
  between operations  14.4 us (2%)
  matrix products  14 us (2%)
    all_to_all x2, blocking collectives, sent_together(): lax.all_to_all(both, axis, split_axis=split_dim, concat_axis=concat_dim,...  143 us
    all_gather x1, blocking collectives, in_one_piece(): lax.all_gather(both, axis, axis=dim, tiled=True)  119 us
    all_to_all x1, blocking collectives, on_device(): lax.all_to_all(send, 'fs', split_axis=0, concat_axis=0, tiled=True)  73.5 us
    all_to_all x1, blocking collectives, sent_to_all(): return lax.all_to_all(copies, axis, split_axis=0, concat_axis=0, tiled=True)  42.3 us
    all_to_all x2, waiting for transfers between devices, sent_to_all(): return lax.all_to_all(copies, axis, split_axis=0, concat_axis=0, tiled=True)  29.1 us
    unnamed x38, local copies, waits for them, and re-layouts  27.7 us
    all_to_all x2, starting transfers between devices, sent_to_all(): return lax.all_to_all(copies, axis, split_axis=0, concat_axis=0, tiled=True)  24 us
    another operation x3, other arithmetic  18.4 us
  transfers between devices with their start and end apart: 5, of which 1 were waited for; matrix products, arithmetic and copies ran while one was open for 9% of the time, Pallas kernels for 0%

profile of v1, /device:TPU:1, one launch (start us, length us, event | category | flops | bytes accessed | tf_op | source)
XLA Modules:
  0.0 593.1 jit_solution(2140871276625205075)
XLA Ops:
  8.4 1.4 fusion.8
  10.1 18.1 %reduce-window.6 = s32[64,12,128]{2,1,0:T(8,128)S(1)} reduce-window(s32[64,12,128]{2,1,0:T(8,128)S(1)} %fusion.32, s32[]{:T(128)} %constant.70.clone.1), window={size=1x1x128 pad=0_0x0_0x127_0}, to_apply=%region_0.0 | reduce-window | flops 12484608 | bytes 786436 | tf_op jit(solution)/shard_map/reduce-window
  29.3 14.6 %scatter_custom_fusion = bf16[2304,2048]{1,0:T(8,128)(2,1)} fusion(s32[1536]{0:T(1024)S(1)} %fusion.35, bf16[]{:T(256)} %constant.72.clone.1, bf16[192,2048]{1,0:T(8,128)(2,1)S(1)} %fusion.9), kind=kCustom, calls=%fused_computation.6 | custom fusion | bytes 10223618 | tf_op jit(solution)/shard_map/scatter | solution.py:111
  43.9 13.1 %reshape.239 = bf16[32,2,1,36,2048]{4,3,1,0,2:T(8,128)(2,1)} reshape(bf16[2304,2048]{1,0:T(8,128)(2,1)} %scatter_custom_fusion) | data formatting | bytes 18874368 | tf_op jit(solution)/shard_map/reshape | solution.py:112
  57.0 1.4 constant_dynamic-slice_fusion
  59.3 73.5 %all_to_all.54 = bf16[32,2,1,36,256]{4,1,3,2,0:T(2,128)(2,1)S(1)} all-to-all(bf16[32,2,1,36,256]{4,1,3,2,0:T(2,128)(2,1)S(1)} %copy.85), channel_id=1, replica_groups=mesh['gr'=2,'fs'=32,'tp'=8] {'fs'}, dimensions={0} | all-to-all | bytes 2359296 | tf_op jit(solution)/shard_map/all_to_all | solution.py:115
  132.8 1.3 copy.86
  135.6 42.3 %all_to_all.55 = bf16[2,1,96,16,256]{4,3,2,1,0:T(8,128)(2,1)S(1)} all-to-all(bf16[2,1,96,16,256]{4,3,2,1,0:T(8,128)(2,1)S(1)} %broadcast_in_dim.10), channel_id=1, replica_groups=mesh['gr'=2,'fs'=32,'tp'=8] {'gr'}, dimensions={0} | all-to-all | bytes 3145728 | tf_op jit(solution)/shard_map/all_to_all | solution.py:12
  178.3 122.1 %all_to_all.56 = bf16[6,32,16,256]{3,2,0,1:T(8,128)(2,1)S(1)} all-to-all(bf16[6,32,16,256]{3,2,0,1:T(8,128)(2,1)S(1)} %copy.73), channel_id=1, replica_groups=mesh['gr'=2,'fs'=32,'tp'=8] {'fs'}, dimensions={1} | all-to-all | bytes 3145728 | tf_op jit(solution)/shard_map/all_to_all | solution.py:36
  301.6 21.3 %all_to_all.57 = bf16[4,1,512,256]{3,0,1,2:T(4,128)(2,1)S(1)} all-to-all(bf16[4,1,512,256]{3,0,1,2:T(4,128)(2,1)S(1)} %copy.77), channel_id=1, replica_groups=mesh['gr'=2,'fs'=32,'tp'=8] {'tp'}, dimensions={2} | all-to-all | bytes 2097152 | tf_op jit(solution)/shard_map/all_to_all | solution.py:36
  326.7 5.9 fusion.11
  332.6 1.5 copy-done.12
  334.0 3.2 fusion.23
  337.4 3.0 broadcast_bitcast_fusion
  340.4 7.9 %reshape.274 = bf16[8,2,73728]{2,1,0:T(2,128)(2,1)} reshape(bf16[8,1,2,36,32,64]{5,4,3,2,1,0:T(8,128)(2,1)} %broadcast_bitcast_fusion) | data formatting | bytes 4718592
  348.3 5.4 all-to-all-start.4
  353.8 29.1 %all-to-all-done.4 = bf16[8,2,73728]{2,1,0:T(2,128)(2,1)} async-done(((bf16[8,2,73728]{2,1,0:T(2,128)(2,1)}), bf16[8,2,73728]{2,1,0:T(2,128)(2,1)}, u32[]{:S(2)}, u32[]{:S(2)}) %all-to-all-start.4) | async-done | bytes 2359328 | tf_op jit(solution)/shard_map/all_to_all | solution.py:12
  383.6 5.7 all-to-all-start.7
  389.4 7.9 %reshape.275 = bf16[8,1,2,36,32,64]{5,4,3,2,1,0:T(8,128)(2,1)} reshape(bf16[8,2,73728]{2,1,0:T(2,128)(2,1)} %all-to-all-done.4) | data formatting | bytes 4718592
  397.3 3.1 bitcast_bitcast_fusion.1
  400.4 5.2 copy.105
  405.6 7.3 %reshape.270 = bf16[32,2,36,512]{3,2,0,1:T(8,128)(2,1)} reshape(bf16[32,2,1,36,8,64]{5,4,3,0,1,2:T(8,128)(2,1)} %copy.105) | data formatting | bytes 4718592 | tf_op jit(solution)/shard_map/reshape.38
  412.9 2.6 fusion.10
  415.5 2.2 copy.91
  417.7 11.9 %all-to-all-start.5 = ((bf16[32,2,1,36,256]{4,1,3,2,0:T(2,128)(2,1)}), bf16[32,2,1,36,256]{4,1,3,2,0:T(2,128)(2,1)S(1)}, u32[]{:S(2)}, u32[]{:S(2)}) async-start(bf16[32,2,1,36,256]{4,1,3,2,0:T(2,128)(2,1)} %copy.91), calls=%async_computation.5 | async-start | bytes 2359296 | tf_op jit(solution)/shard_map/all_to_all | solution.py:124
  430.8 119.5 %all_gather.7 = bf16[2048,128]{1,0:T(8,128)(2,1)S(1)} all-gather(bf16[64,128]{1,0:T(8,128)(2,1)S(1)} %pad_maximum_fusion.2), channel_id=1, replica_groups=mesh['gr'=2,'fs'=32,'tp'=8] {'fs'}, dimensions={0}, use_global_device_ids=true | all-gather | bytes 540672 | tf_op jit(solution)/shard_map/all_gather | solution.py:42
  550.2 1.1 fusion.43
  551.4 1.9 copy.98
  553.3 1.9 copy.99
  559.2 18.6 %all-to-all-start.6 = ((bf16[8,192,64]{1,2,0:T(8,128)(2,1)}), bf16[8,192,64]{1,2,0:T(8,128)(2,1)S(1)}, u32[]{:S(2)}, u32[]{:S(2)}) async-start(bf16[8,192,64]{1,2,0:T(8,128)(2,1)} %broadcast_in_dim.27), calls=%async_computation.6 | async-start | bytes 524288 | tf_op jit(solution)/shard_map/all_to_all | solution.py:12
  577.8 1.5 copy.92
  579.5 4.8 gather_fusion
  (84 shorter events, 18.4 us)
Async XLA Ops:
  7.2 2.6 copy-start.1
  7.2 319.5 %all-gather.2.cloned.1.call-start = ((), (), s32[]{:S(2)}) async-start(), calls=%async_computation.8 | async-start | bytes 11796480 | tf_op jit(solution)/shard_map/all_gather | solution.py:116
  132.8 1.3 copy-start.3
  134.0 1.0 copy-start.6
  134.0 1.2 copy-start.7
  326.7 5.9 copy-start.5
  326.7 7.3 %copy-start.12 = (bf16[32,2,1,36,2048]{4,3,0,1,2:T(8,128)(2,1)S(1)}, bf16[32,2,1,36,2048]{4,3,0,1,2:T(8,128)(2,1)}, u32[]{:S(2)}) copy-start(bf16[32,2,1,36,2048]{4,3,0,1,2:T(8,128)(2,1)} %all-gather.2.cloned.1.call-done) | copy-start | bytes 28311556
  348.3 5.4 copy-start.10
  348.3 34.6 %all-to-all-start.4 = ((bf16[8,2,73728]{2,1,0:T(2,128)(2,1)}), bf16[8,2,73728]{2,1,0:T(2,128)(2,1)}, u32[]{:S(2)}, u32[]{:S(2)}) async-start(bf16[8,2,73728]{2,1,0:T(2,128)(2,1)} %reshape.274), calls=%async_computation.4 | async-start | bytes 4718592 | tf_op jit(solution)/shard_map/all_to_all | solution.py:12
  383.6 34.1 %all-to-all-start.7 = ((bf16[32,16,256]{2,1,0:T(8,128)(2,1)}), bf16[32,16,256]{2,1,0:T(8,128)(2,1)S(1)}, u32[]{:S(2)}, u32[]{:S(2)}) async-start(bf16[32,16,256]{2,1,0:T(8,128)(2,1)} %stack.2), calls=%async_computation.7 | async-start | bytes 524288 | tf_op jit(solution)/shard_map/all_to_all | solution.py:83
  389.4 23.5 %copy-start.4 = (bf16[2,32,16,256]{3,2,1,0:T(8,128)(2,1)}, bf16[2,32,16,256]{3,2,1,0:T(8,128)(2,1)S(1)}, u32[]{:S(2)}) copy-start(bf16[2,32,16,256]{3,2,1,0:T(8,128)(2,1)S(1)} %copy.107) | copy-start | bytes 1572868
  417.7 12.7 %copy-start.11 = (f32[192,8]{0,1:T(8,128)S(1)}, f32[192,8]{0,1:T(8,128)}, u32[]{:S(2)}) copy-start(f32[192,8]{0,1:T(8,128)} %param.12) | copy-start | bytes 18436
  417.7 12.9 %copy-start.8 = (f32[64,64]{1,0:T(8,128)S(1)}, f32[64,64]{1,0:T(8,128)}, u32[]{:S(2)}) copy-start(f32[64,64]{1,0:T(8,128)} %param.17) | copy-start | bytes 49156
  417.7 12.9 %copy-start.9 = (f32[64,64]{1,0:T(8,128)S(1)}, f32[64,64]{1,0:T(8,128)}, u32[]{:S(2)}) copy-start(f32[64,64]{1,0:T(8,128)} %param.18) | copy-start | bytes 49156
  417.7 140.3 %all-to-all-start.5 = ((bf16[32,2,1,36,256]{4,1,3,2,0:T(2,128)(2,1)}), bf16[32,2,1,36,256]{4,1,3,2,0:T(2,128)(2,1)S(1)}, u32[]{:S(2)}, u32[]{:S(2)}) async-start(bf16[32,2,1,36,256]{4,1,3,2,0:T(2,128)(2,1)} %copy.91), calls=%async_computation.5 | async-start | bytes 2359296 | tf_op jit(solution)/shard_map/all_to_all | solution.py:124
  555.2 1.1 copy-start.2
  558.0 1.1 copy-start
  559.2 25.5 %all-to-all-start.6 = ((bf16[8,192,64]{1,2,0:T(8,128)(2,1)}), bf16[8,192,64]{1,2,0:T(8,128)(2,1)S(1)}, u32[]{:S(2)}, u32[]{:S(2)}) async-start(bf16[8,192,64]{1,2,0:T(8,128)(2,1)} %broadcast_in_dim.27), calls=%async_computation.6 | async-start | bytes 524288 | tf_op jit(solution)/shard_map/all_to_all | solution.py:12
Sparse Core Ops, SparseCore 0:
  134.2 66.9 all-gather.1
